TPU v7x, 32 devices: a whole 2x2x4 slice. The times are simulated.
32 devices in a mesh: sp: 4 (over z), fs: 4 (over y, x), tp: 2 (over core).
Axes of the slice: x: 2, y: 2, z: 4, core: 2. Of those that a mesh axis runs over, the one named last changes fastest.
Arguments:
- tokens: bfloat16 [4, 1024, 2048], P('fs', 'sp'), may hold values from -6 to 6
- norm_gain: float32 [2048], replicated, may hold values from 0.1 to 1.9
- query_weight: bfloat16 [2048, 1024], P(('sp', 'fs'), 'tp'), may hold values from -0.125 to 0.125
- key_weight: bfloat16 [2048, 1024], P(('sp', 'fs'), 'tp'), may hold values from -0.125 to 0.125
- value_weight: bfloat16 [2048, 1024], P(('sp', 'fs'), 'tp'), may hold values from -0.125 to 0.125
- outgate_weight: bfloat16 [2048, 1024], P(('sp', 'fs'), 'tp'), may hold values from -0.125 to 0.125
- gate_weight: bfloat16 [4, 8, 2048], P(None, 'tp'), may hold values from -0.125 to 0.125
- gate_bias: float32 [4, 8], P(None, 'tp'), may hold values from -1 to 100
- decay_extra: float32 [4, 2, 8, 1024], P('fs', None, 'tp', 'sp'), may hold values from -0.75 to 0
- init_memory: float32 [4, 2, 8, 128, 128], P('fs', None, 'tp'), may hold values from -48 to 48
- init_normalizer: float32 [4, 2, 8, 128], P('fs', None, 'tp'), may hold values from -48 to 48
- head_gain: float32 [8, 128], P('tp'), may hold values from 0.1 to 1.9
- pool_weight: bfloat16 [2048, 2048], P(('sp', 'fs'), 'tp'), may hold values from -0.125 to 0.125
- mem_out_weight: bfloat16 [2048, 1024], P(('sp', 'fs'), 'tp'), may hold values from -0.1875 to 0.1875
- pool_out_weight: bfloat16 [2048, 2048], P(('sp', 'fs'), 'tp'), may hold values from -0.125 to 0.125
Outputs:
- mixed: bfloat16 [4, 1024, 2048], P('fs', ('sp', 'tp'))
All inputs are finite; a program needn't handle non-finite values.
Results may differ from a plain program's by a relative error of at most 0.014.
Values may be sent and summed in bfloat16 or wider, within the bound.
A program may use at most 64 MiB of HBM per device.

v0:
```python
import math
import jax
import jax.numpy as jnp
from jax import lax
from jax.sharding import PartitionSpec as P

HALO = 8
norm_eps = 1e-06
exact_mode = lax.Precision.HIGHEST


def carried_in(x, axis, combine, identity, reverse):
    length, position = (lax.axis_size(axis), lax.axis_index(axis))
    everything = jax.tree.map(lambda part: lax.all_gather(part, axis), x)
    start = jax.tree.map(
        lambda part, zero: jnp.broadcast_to(jnp.asarray(zero, part.dtype), part.shape), x, identity
    )

    def lap(k, before):
        at = length - 1 - k if reverse else k
        reached = at > position if reverse else at < position
        new = combine(before, jax.tree.map(lambda part: part[at], everything))
        return jax.tree.map(lambda a, b: jnp.where(reached, a, b), new, before)

    return lax.fori_loop(0, length, lap, start)


def padded_2(block, sides, width):
    for axis, dim in sides:
        count = lax.axis_size(axis)
        forward = [(i, i + 1) for i in range(count - 1)]
        backward = [(target, source) for source, target in forward]
        low = lax.ppermute(
            lax.slice_in_dim(block, block.shape[dim] - width, None, axis=dim), axis, forward
        )
        high = lax.ppermute(lax.slice_in_dim(block, 0, width, axis=dim), axis, backward)
        block = jnp.concatenate([low, block, high], axis=dim)
    return block


def block_output(
    query_rows, key_rows, value_rows, input_gate, log_forget, memory, normalizer, stabilizer
):
    block_len = query_rows.shape[1]
    key_scale = key_rows.shape[-1] ** (-0.5)
    lower_mask = jnp.tril(jnp.ones((block_len, block_len), dtype=bool))
    summed = jnp.cumsum(log_forget, axis=-1)
    log_decay = jnp.where(
        lower_mask, summed[:, :, None] - summed[:, None, :] + input_gate[:, None, :], -jnp.inf
    )
    log_carry = stabilizer[:, None] + summed
    running_max = jnp.maximum(log_carry, jnp.max(log_decay, axis=-1))
    scores = (
        jnp.einsum("btd,bsd->bts", query_rows, key_rows, preferred_element_type=jnp.float32)
        * key_scale
    )
    inner_weight = jnp.exp(log_decay - running_max[:, :, None]) * scores
    weight_rounded = inner_weight.astype(jnp.bfloat16)
    carry_weight = jnp.exp(log_carry - running_max)
    query_wide = query_rows.astype(jnp.float32)
    numerator = carry_weight[:, :, None] * jnp.einsum(
        "bed,btd->bte", memory, query_wide, precision=exact_mode
    )
    numerator = numerator + jnp.einsum(
        "bts,bse->bte", weight_rounded, value_rows, preferred_element_type=jnp.float32
    )
    denominator = carry_weight * jnp.einsum(
        "bd,btd->bt", normalizer, query_wide, precision=exact_mode
    )
    denominator = denominator + jnp.sum(inner_weight, axis=-1)
    return numerator / jnp.maximum(jnp.abs(denominator), jnp.exp(-running_max))[:, :, None]


def block_summary(key_rows, value_rows, input_gate, log_forget):
    key_wide = key_rows.astype(jnp.float32) * key_rows.shape[-1] ** (-0.5)
    summed = jnp.cumsum(log_forget, axis=-1)
    forget_total = summed[:, -1]
    log_weight = forget_total[:, None] - summed + input_gate
    running_max = jnp.max(log_weight, axis=-1)
    weights = jnp.exp(log_weight - running_max[:, None])
    memory = jnp.einsum(
        "bse,bsd->bed",
        weights[:, :, None] * value_rows.astype(jnp.float32),
        key_wide,
        precision=exact_mode,
    )
    normalizer = jnp.einsum("bs,bsd->bd", weights, key_wide, precision=exact_mode)
    return (memory, normalizer, running_max, forget_total)


def combine(earlier, latter):
    early_memory, early_norm, early_max, early_total = earlier
    late_memory, late_norm, late_max, late_total = latter
    joint_max = jnp.maximum(early_max + late_total, late_max)
    early_scale = jnp.exp(early_max + late_total - joint_max)
    late_scale = jnp.exp(late_max - joint_max)
    memory = early_scale[:, None, None] * early_memory + late_scale[:, None, None] * late_memory
    normalizer = early_scale[:, None] * early_norm + late_scale[:, None] * late_norm
    return (memory, normalizer, joint_max, early_total + late_total)


def span_sweep(
    query_rows, key_rows, value_rows, input_gate, log_forget, memory, normalizer, stabilizer, span
):
    block_count = query_rows.shape[1] // span

    def to_blocks(array):
        shaped = array.reshape((array.shape[0], block_count, span) + array.shape[2:])
        return jnp.moveaxis(shaped, 1, 0)

    def advance(carried, pieces):
        query_blk, key_blk, value_blk, gate_blk, forget_blk = pieces
        result = block_output(
            query_blk, key_blk, value_blk, gate_blk, forget_blk, carried[0], carried[1], carried[2]
        )
        return (combine(carried, block_summary(key_blk, value_blk, gate_blk, forget_blk)), result)

    initial = (memory, normalizer, stabilizer, jnp.zeros_like(stabilizer))
    ignored, outputs = lax.scan(
        advance,
        initial,
        tuple(
            (
                to_blocks(array)
                for array in (query_rows, key_rows, value_rows, input_gate, log_forget)
            )
        ),
    )
    return jnp.moveaxis(outputs, 0, 1).reshape(query_rows.shape[:2] + (value_rows.shape[2],))


def reverse_time(array):
    return jnp.flip(array, axis=1)


def to_heads(matrix, head_count):
    shaped = matrix.reshape(matrix.shape[0], head_count, matrix.shape[1] // head_count)
    return shaped.transpose(1, 0, 2)


def pool_window(padded, positions, channels, seq_len, group_size):
    row_count = positions.shape[0]
    group_index = channels // group_size
    reach_left = jnp.left_shift(jnp.ones_like(group_index), group_index)
    reach_right = reach_left - 1
    window_sum = jnp.zeros((row_count, channels.shape[0]), jnp.float32)
    for offset in range(-HALO, HALO):
        inside = ((offset >= -reach_left) & (offset <= reach_right)).astype(jnp.float32)
        window_sum = window_sum + inside * padded[HALO + offset : HALO + offset + row_count]
    first_pos = jnp.maximum(positions[:, None] - reach_left[None, :], 0)
    last_pos = jnp.minimum(positions[:, None] + reach_right[None, :], seq_len - 1)
    counted = (last_pos - first_pos + 1).astype(jnp.float32)
    centre = padded[HALO : HALO + row_count]
    return (window_sum / counted - centre).astype(jnp.bfloat16)


def per_device(
    tokens,
    norm_gain,
    query_weight,
    key_weight,
    value_weight,
    outgate_weight,
    gate_weight,
    gate_bias,
    decay_extra,
    init_memory,
    init_normalizer,
    head_gain,
    pool_weight,
    mem_out_weight,
    pool_out_weight,
):
    block_len = tokens.shape[1]
    model_width = tokens.shape[2]
    head_count, head_width = head_gain.shape
    span = math.gcd(block_len, 256)
    flattened = tokens[0].astype(jnp.float32)
    normed = (
        flattened
        * lax.rsqrt(jnp.mean(flattened * flattened, axis=-1, keepdims=True) + norm_eps)
        * norm_gain
    ).astype(jnp.bfloat16)
    zero_start = tuple(
        (
            jnp.zeros((block_len, weight.shape[1]), jnp.float32)
            for weight in (query_weight, key_weight, value_weight, outgate_weight, pool_weight)
        )
    )
    zero_start = zero_start + (
        jnp.zeros((model_width, mem_out_weight.shape[1]), jnp.bfloat16),
        jnp.zeros((model_width, pool_out_weight.shape[1]), jnp.bfloat16),
    )
    line_query, line_key, line_value, line_outgate, line_pool, line_mem_out, line_pool_out = (
        lax.all_gather(query_weight, "fs", axis=0, tiled=True),
        lax.all_gather(key_weight, "fs", axis=0, tiled=True),
        lax.all_gather(value_weight, "fs", axis=0, tiled=True),
        lax.all_gather(outgate_weight, "fs", axis=0, tiled=True),
        lax.all_gather(pool_weight, "fs", axis=0, tiled=True),
        lax.all_gather(mem_out_weight, "fs", axis=0, tiled=True),
        lax.all_gather(pool_out_weight, "fs", axis=0, tiled=True),
    )
    pieces = (
        lax.all_gather(line_query, "sp", axis=0, tiled=True),
        lax.all_gather(line_key, "sp", axis=0, tiled=True),
        lax.all_gather(line_value, "sp", axis=0, tiled=True),
        lax.all_gather(line_outgate, "sp", axis=0, tiled=True),
        lax.all_gather(line_pool, "sp", axis=0, tiled=True),
        lax.all_gather(line_mem_out, "sp", axis=0, tiled=True),
        lax.all_gather(line_pool_out, "sp", axis=0, tiled=True),
    )
    partial_sums = tuple(
        (
            jnp.dot(normed, weight_rows, preferred_element_type=jnp.float32)
            for weight_rows in pieces[:5]
        )
    )
    collected = tuple((weight_rows for weight_rows in pieces[5:]))
    folded = partial_sums + collected
    query_proj, key_proj, value_proj, outgate, pool_input = tuple(
        (running.astype(jnp.bfloat16) for running in folded[:5])
    )
    mem_weight_all = folded[5]
    pool_weight_all = folded[6]
    gate_pre = lax.dot_general(
        normed,
        gate_weight.reshape(4 * head_count, model_width),
        (((1,), (1,)), ((), ())),
        preferred_element_type=jnp.float32,
    ) + gate_bias.reshape(4 * head_count)
    gate_pre = gate_pre.reshape(block_len, 4, head_count).transpose(1, 2, 0)
    query_heads = to_heads(query_proj, head_count)
    key_heads = to_heads(key_proj, head_count)
    value_heads = to_heads(value_proj, head_count)
    forward_forget = jax.nn.log_sigmoid(gate_pre[1]) + decay_extra[0, 0]
    backward_forget = jax.nn.log_sigmoid(gate_pre[3]) + decay_extra[0, 1]
    zero_rows = jnp.zeros((head_count,), jnp.float32)
    identity = (
        jnp.zeros((head_count, head_width, head_width), jnp.float32),
        jnp.zeros((head_count, head_width), jnp.float32),
        jnp.full((head_count,), -1e30, jnp.float32),
        zero_rows,
    )
    front_memory, front_norm, front_max, front_total = block_summary(
        key_heads, value_heads, gate_pre[0], forward_forget
    )
    prefix = carried_in(
        (front_memory, front_norm, front_max, front_total), "sp", combine, identity, False
    )
    incoming = combine((init_memory[0, 0], init_normalizer[0, 0], zero_rows, zero_rows), prefix)
    forward_out = span_sweep(
        query_heads,
        key_heads,
        value_heads,
        gate_pre[0],
        forward_forget,
        incoming[0],
        incoming[1],
        incoming[2],
        span,
    )
    back_query = reverse_time(query_heads)
    back_key = reverse_time(key_heads)
    back_value = reverse_time(value_heads)
    back_gate = reverse_time(gate_pre[2])
    back_forget = reverse_time(backward_forget)
    rear_memory, rear_norm, rear_max, rear_total = block_summary(
        back_key, back_value, back_gate, back_forget
    )
    suffix = carried_in(
        (rear_memory, rear_norm, rear_max, rear_total), "sp", combine, identity, True
    )
    back_incoming = combine(
        (init_memory[0, 1], init_normalizer[0, 1], zero_rows, zero_rows), suffix
    )
    backward_out = reverse_time(
        span_sweep(
            back_query,
            back_key,
            back_value,
            back_gate,
            back_forget,
            back_incoming[0],
            back_incoming[1],
            back_incoming[2],
            span,
        )
    )
    summed_dirs = (forward_out + backward_out).transpose(1, 0, 2)
    normed_heads = (
        summed_dirs
        * lax.rsqrt(jnp.mean(summed_dirs * summed_dirs, axis=-1, keepdims=True) + norm_eps)
        * head_gain
    )
    out_gate = jax.nn.sigmoid(
        outgate.astype(jnp.float32).reshape(block_len, head_count, head_width)
    )
    memory_out = (
        (normed_heads * out_gate).astype(jnp.bfloat16).reshape(block_len, head_count * head_width)
    )
    padded = padded_2(pool_input, (("sp", 0),), HALO).astype(jnp.float32)
    feature_count = pool_input.shape[1]
    positions = lax.axis_index("sp") * block_len + jnp.arange(block_len, dtype=jnp.int32)
    channels = lax.axis_index("tp") * feature_count + jnp.arange(feature_count, dtype=jnp.int32)
    pool_out = pool_window(
        padded, positions, channels, block_len * lax.axis_size("sp"), model_width // 4
    )
    own_rows = block_len // lax.axis_size("tp")
    result = lax.dot_general(
        memory_out, mem_weight_all, (((1,), (1,)), ((), ())), preferred_element_type=jnp.float32
    )
    mixed = lax.psum_scatter(
        (
            result
            + lax.dot_general(
                pool_out,
                pool_weight_all,
                (((1,), (1,)), ((), ())),
                preferred_element_type=jnp.float32,
            )
        ).astype(jnp.bfloat16),
        "tp",
        scatter_dimension=0,
        tiled=True,
    )
    return mixed.reshape(1, own_rows, model_width)


def solution(mesh):
    placed = (
        P("fs", "sp", None),
        P(),
        P(("sp", "fs"), "tp"),
        P(("sp", "fs"), "tp"),
        P(("sp", "fs"), "tp"),
        P(("sp", "fs"), "tp"),
        P(None, "tp", None),
        P(None, "tp"),
        P("fs", None, "tp", "sp"),
        P("fs", None, "tp", None, None),
        P("fs", None, "tp", None),
        P("tp", None),
        P(("sp", "fs"), "tp"),
        P(("sp", "fs"), "tp"),
        P(("sp", "fs"), "tp"),
    )
    return jax.shard_map(
        per_device,
        mesh=mesh,
        in_specs=placed,
        out_specs=P("fs", ("sp", "tp"), None),
        check_vma=False,
    )
```

profile of v0, /device:TPU:0, one launch (start us, length us, event | category | flops | bytes accessed | tf_op | source)
XLA Modules:
  0.0 544.0 jit_solution(11762868126986876266)
XLA Ops:
  6.5 13.3 %all_gather.89 = bf16[512,512]{1,0:T(8,128)(2,1)} all-gather(bf16[128,512]{1,0:T(8,128)(2,1)} %param.22), channel_id=1, replica_groups=mesh['sp'=4,'fs'=4,'tp'=2] {'fs'}, dimensions={0}, use_global_device_ids=true | all-gather | bytes 655360 | tf_op jit(solution)/shard_map/all_gather | solution.py:196
  19.9 11.6 %all_gather.87 = bf16[512,512]{1,0:T(8,128)(2,1)} all-gather(bf16[128,512]{1,0:T(8,128)(2,1)} %param.23), channel_id=1, replica_groups=mesh['sp'=4,'fs'=4,'tp'=2] {'fs'}, dimensions={0}, use_global_device_ids=true | all-gather | bytes 655360 | tf_op jit(solution)/shard_map/all_gather | solution.py:197
  31.6 0.7 all-gather.32.cloned.1.call-update
  32.9 10.5 %all_gather.95 = bf16[512,512]{1,0:T(8,128)(2,1)} all-gather(bf16[128,512]{1,0:T(8,128)(2,1)S(1)} %copy-done.3), channel_id=1, replica_groups=mesh['sp'=4,'fs'=4,'tp'=2] {'fs'}, dimensions={0}, use_global_device_ids=true | all-gather | bytes 655360 | tf_op jit(solution)/shard_map/all_gather | solution.py:195
  43.5 10.5 %all_gather.104 = bf16[512,512]{1,0:T(8,128)(2,1)} all-gather(bf16[128,512]{1,0:T(8,128)(2,1)S(1)} %copy-done.4), channel_id=1, replica_groups=mesh['sp'=4,'fs'=4,'tp'=2] {'fs'}, dimensions={0}, use_global_device_ids=true | all-gather | bytes 655360 | tf_op jit(solution)/shard_map/all_gather | solution.py:198
  55.1 1.2 reduce-window.24
  57.2 8.7 %all-gather.24.cloned.1.call-done = bf16[2048,512]{1,0:T(8,128)(2,1)} async-done(((bf16[512,512]{1,0:T(8,128)(2,1)}), bf16[2048,512]{1,0:T(8,128)(2,1)}) %all-gather.24.cloned.1.call-update) | async-done | bytes 2097168 | tf_op jit(solution)/shard_map/all_gather | solution.py:205
  65.9 2.3 fusion.36
  68.3 43.7 %all-gather.22.cloned.1.call-done = bf16[2048,512]{1,0:T(8,128)(2,1)} async-done(((bf16[512,512]{1,0:T(8,128)(2,1)}), bf16[2048,512]{1,0:T(8,128)(2,1)}) %all-gather.22.cloned.1.call-update) | async-done | bytes 2097168 | tf_op jit(solution)/shard_map/all_gather | solution.py:206
  112.0 2.3 fusion.35
  114.3 1.9 fusion.71
  116.5 1.2 reduce-window.26
  119.5 1.9 fusion.65
  121.5 17.7 %all-gather.32.cloned.1.call-done = bf16[512,1024]{1,0:T(8,128)(2,1)} async-done(((bf16[128,1024]{1,0:T(8,128)(2,1)}), bf16[512,1024]{1,0:T(8,128)(2,1)}) %all-gather.32.cloned.1.call-update) | async-done | bytes 1048592 | tf_op jit(solution)/shard_map/all_gather | solution.py:199
  139.3 28.2 %all-gather.36.cloned.1.call-done = bf16[512,1024]{1,0:T(8,128)(2,1)} async-done(((bf16[128,1024]{1,0:T(8,128)(2,1)}), bf16[512,1024]{1,0:T(8,128)(2,1)}) %all-gather.36.cloned.1.call-update) | async-done | bytes 1048592 | tf_op jit(solution)/shard_map/all_gather | solution.py:201
  167.5 10.6 %all_gather.106 = bf16[512,512]{1,0:T(8,128)(2,1)} all-gather(bf16[128,512]{1,0:T(8,128)(2,1)S(1)} %copy-done.5), channel_id=1, replica_groups=mesh['sp'=4,'fs'=4,'tp'=2] {'fs'}, dimensions={0}, use_global_device_ids=true | all-gather | bytes 655360 | tf_op jit(solution)/shard_map/all_gather | solution.py:200
  180.2 0.6 and_convert_fusion.4
  180.8 0.6 and_convert_fusion.6
  181.4 0.6 and_convert_fusion.8
  182.6 0.6 and_convert_fusion.12
  185.9 12.3 %all-reduce.4 = (f32[16]{0:T(128)S(1)}, f32[16]{0:T(128)S(1)}, f32[16]{0:T(128)S(1)}, f32[16]{0:T(128)S(1)}) all-reduce(f32[16]{0:T(128)S(1)} %dynamic-update-slice.2, f32[16]{0:T(128)S(1)} %dynamic-update-slice.3, f32[16]{0:T(128)S(1)} %dynamic-update-slice, f32[16]{0:T(128)S(1)} %dynamic-update-slice.1), channel_id=6, replica_groups=mesh['sp'=4,'fs'=4,'tp'=2] {'sp'}, use_global_device_ids=true, to_apply=%add.2 | all-reduce | flops 64 | bytes 512
  198.2 0.7 reshape.473
  199.0 0.7 reshape.477
  200.2 0.7 fusion.58
  201.4 12.5 %all-gather.8 = f32[4,4,128]{2,1,0:T(4,128)S(1)} all-gather(f32[1,4,128]{2,1,0:T(4,128)S(1)} %bitcast.306), channel_id=5, replica_groups=mesh['sp'=4,'fs'=4,'tp'=2] {'sp'}, dimensions={0}, use_global_device_ids=true | all-gather | bytes 10240 | tf_op jit(solution)/shard_map/all_gather | solution.py:14
  214.2 12.1 %all-gather.9 = f32[4,4,128]{2,1,0:T(4,128)S(1)} all-gather(f32[1,4,128]{2,1,0:T(4,128)S(1)} %bitcast.302), channel_id=9, replica_groups=mesh['sp'=4,'fs'=4,'tp'=2] {'sp'}, dimensions={0}, use_global_device_ids=true | all-gather | bytes 10240 | tf_op jit(solution)/shard_map/all_gather | solution.py:14
  226.4 2.3 fusion.37
  229.1 31.8 %all-gather.28.cloned.1.call-done = bf16[2048,512]{1,0:T(8,128)(2,1)} async-done(((bf16[512,512]{1,0:T(8,128)(2,1)}), bf16[2048,512]{1,0:T(8,128)(2,1)}) %all-gather.28.cloned.1.call-update) | async-done | bytes 2097168 | tf_op jit(solution)/shard_map/all_gather | solution.py:207
  260.9 3.2 fusion.34
  264.1 1.2 copy.60
  265.4 23.9 %all-gather.40.cloned.1.call-done = f32[16,128,128]{2,1,0:T(8,128)} async-done(((f32[4,128,128]{2,1,0:T(8,128)}), f32[16,128,128]{2,1,0:T(8,128)}) %all-gather.40.cloned.1.call-update) | async-done | bytes 1048592 | tf_op jit(solution)/shard_map/all_gather | solution.py:14
  289.3 7.4 %while.12 = (s32[]{:T(128)}, f32[4,128,128]{2,1,0:T(8,128)S(1)}, f32[4,128]{1,0:T(4,128)S(1)}, f32[4]{0:T(128)S(1)}, f32[4]{0:T(128)S(1)}, /*index=5*/s32[]{:T(1...) while((s32[]{:T(128)}, f32[4,128,128]{2,1,0:T(8,128)S(1)}, ...), condition=%wide.region_5.6_spmd.clone, body=%wide.region_4.5_spmd.clone.sunk | while | flops 330284 | bytes 792973 | solution.py:25
  289.3 0.7 broadcast_select_fusion.10
  290.0 1.1 fusion.157
  291.1 0.7 broadcast_select_fusion.10
  291.8 1.1 fusion.157
  293.0 0.7 broadcast_select_fusion.10
  293.7 1.1 fusion.157
  294.9 0.7 broadcast_select_fusion.10
  295.5 1.1 fusion.157
  297.8 2.3 fusion.133
  300.1 18.2 %all-gather.42.cloned.1.call-done = f32[16,128,128]{2,1,0:T(8,128)} async-done(((f32[4,128,128]{2,1,0:T(8,128)}), f32[16,128,128]{2,1,0:T(8,128)}) %all-gather.42.cloned.1.call-update) | async-done | bytes 1048592 | tf_op jit(solution)/shard_map/all_gather | solution.py:14
  318.3 7.5 %while.13 = (s32[]{:T(128)}, f32[4,128,128]{2,1,0:T(8,128)S(1)}, f32[4,128]{1,0:T(4,128)S(1)}, f32[4]{0:T(128)S(1)}, f32[4]{0:T(128)S(1)}, /*index=5*/s32[]{:T(1...) while((s32[]{:T(128)}, f32[4,128,128]{2,1,0:T(8,128)S(1)}, ...), condition=%wide.region_12.13_spmd.clone, body=%wide.region_11.12_spmd.clone.sunk | while | flops 330288 | bytes 793035 | solution.py:25
  318.3 0.7 broadcast_select_fusion.11
  319.0 1.1 fusion.159
  320.2 0.7 broadcast_select_fusion.11
  320.9 1.1 fusion.159
  322.0 0.7 broadcast_select_fusion.11
  322.7 1.1 fusion.159
  323.9 0.7 broadcast_select_fusion.11
  324.6 1.1 fusion.159
  327.7 1.2 fusion.25
  329.0 5.0 rev.26
  334.4 1.7 multiply_reduce_fusion
  336.1 63.9 %all-gather.34.cloned.1.call-done = bf16[2048,1024]{1,0:T(8,128)(2,1)} async-done(((bf16[512,1024]{1,0:T(8,128)(2,1)}), bf16[2048,1024]{1,0:T(8,128)(2,1)}) %all-gather.34.cloned.1.call-update) | async-done | bytes 4194320 | tf_op jit(solution)/shard_map/all_gather | solution.py:208
  400.0 3.5 convolution_convert_fusion
  403.7 1.3 collective-permute-start
  405.0 1.3 collective-permute-start.1
  406.4 4.2 collective-permute-done.1
  410.8 69.9 %all-gather.38.cloned.1.call-done = bf16[2048,1024]{1,0:T(8,128)(2,1)} async-done(((bf16[512,1024]{1,0:T(8,128)(2,1)}), bf16[2048,1024]{1,0:T(8,128)(2,1)}) %all-gather.38.cloned.1.call-update) | async-done | bytes 4194320 | tf_op jit(solution)/shard_map/all_gather | solution.py:210
  480.8 5.3 fusion.74
  486.1 40.3 %all-gather.30.cloned.1.call-done = bf16[2048,512]{1,0:T(8,128)(2,1)} async-done(((bf16[512,512]{1,0:T(8,128)(2,1)}), bf16[2048,512]{1,0:T(8,128)(2,1)}) %all-gather.30.cloned.1.call-update) | async-done | bytes 2097168 | tf_op jit(solution)/shard_map/all_gather | solution.py:209
  526.4 3.4 fusion.16
  529.8 7.3 %reduce-scatter.2.cloned.1.call-done = bf16[128,2048]{1,0:T(8,128)(2,1)} async-done(((bf16[256,2048]{1,0:T(8,128)(2,1)}), bf16[128,2048]{1,0:T(8,128)(2,1)}) %reduce-scatter.2.cloned.1.call-update) | async-done | bytes 524304 | tf_op jit(solution)/shard_map/reduce_scatter | solution.py:312
  (204 shorter events, 15.7 us)
Async XLA Ops:
  6.5 26.4 %copy-start.3 = (bf16[128,512]{1,0:T(8,128)(2,1)S(1)}, bf16[128,512]{1,0:T(8,128)(2,1)}, u32[]{:S(2)}) copy-start(bf16[128,512]{1,0:T(8,128)(2,1)} %param.21) | copy-start | bytes 393220
  6.5 37.0 %copy-start.4 = (bf16[128,512]{1,0:T(8,128)(2,1)S(1)}, bf16[128,512]{1,0:T(8,128)(2,1)}, u32[]{:S(2)}) copy-start(bf16[128,512]{1,0:T(8,128)(2,1)} %param.24) | copy-start | bytes 393220
  6.5 59.4 %all-gather.24.cloned.1.call-start = ((), (), s32[]{:S(2)}) async-start(), calls=%async_computation.2 | async-start | bytes 2621440 | tf_op jit(solution)/shard_map/all_gather | solution.py:205
  19.9 34.3 %copy-start.6 = (bf16[4,4,2048]{2,1,0:T(4,128)(2,1)S(1)}, bf16[4,4,2048]{2,1,0:T(4,128)(2,1)}, u32[]{:S(2)}) copy-start(bf16[4,4,2048]{2,1,0:T(4,128)(2,1)} %param.25) | copy-start | bytes 196612
  19.9 34.3 %copy-start.28 = (f32[4,4]{1,0:T(4,128)S(1)}, f32[4,4]{1,0:T(4,128)}, u32[]{:S(2)}) copy-start(f32[4,4]{1,0:T(4,128)} %param.26) | copy-start | bytes 196
  19.9 34.4 %copy-start = (bf16[1,256,2048]{2,1,0:T(8,128)(2,1)S(1)}, bf16[1,256,2048]{2,1,0:T(8,128)(2,1)}, u32[]{:S(2)}) copy-start(bf16[1,256,2048]{2,1,0:T(8,128)(2,1)} %param.19) | copy-start | bytes 3145732
  19.9 92.1 %all-gather.22.cloned.1.call-start = ((), (), s32[]{:S(2)}) async-start(), calls=%async_computation.1 | async-start | bytes 2621440 | tf_op jit(solution)/shard_map/all_gather | solution.py:206
  31.5 23.0 %copy-start.34 = (f32[2048]{0:T(1024)S(1)}, f32[2048]{0:T(1024)}, u32[]{:S(2)}) copy-start(f32[2048]{0:T(1024)} %param.20) | copy-start | bytes 24580
  31.5 107.7 %all-gather.32.cloned.1.call-start = ((), (), s32[]{:S(2)}) async-start(), calls=%async_computation.6 | async-start | bytes 1310720 | tf_op jit(solution)/shard_map/all_gather | solution.py:199
  32.3 135.2 %all-gather.36.cloned.1.call-start = ((), (), s32[]{:S(2)}) async-start(), calls=%async_computation.8 | async-start | bytes 1310720 | tf_op jit(solution)/shard_map/all_gather | solution.py:201
  32.8 193.5 %all-gather.26.cloned.1.call-start = ((), (), s32[]{:S(2)}) async-start(), calls=%async_computation.3 | async-start | bytes 2621440 | tf_op jit(solution)/shard_map/all_gather | solution.py:204
  43.4 11.7 %slice-start = ((f32[1,2,4,256]{3,2,1,0:T(4,128)}), f32[1,1,4,256]{3,2,1,0:T(4,128)S(1)}, s32[]{:S(2)}) async-start(f32[1,2,4,256]{3,2,1,0:T(4,128)} %param.27), calls=%async_computation.13 | async-start | bytes 8192 | tf_op jit(solution)/shard_map/slice | solution.py:235
  43.4 13.7 %copy-start.7 = (f32[1,2,4,256]{3,2,1,0:T(4,128)S(1)}, f32[1,2,4,256]{3,2,1,0:T(4,128)}, u32[]{:S(2)}) copy-start(f32[1,2,4,256]{3,2,1,0:T(4,128)} %param.27) | copy-start | bytes 24580
  43.5 217.5 %all-gather.28.cloned.1.call-start = ((), (), s32[]{:S(2)}) async-start(), calls=%async_computation.4 | async-start | bytes 2621440 | tf_op jit(solution)/shard_map/all_gather | solution.py:207
  54.1 235.2 %all-gather.40.cloned.1.call-start = ((), (), s32[]{:S(2)}) async-start(), calls=%async_computation.11 | async-start | bytes 1310720 | tf_op jit(solution)/shard_map/all_gather | solution.py:14
  54.6 206.3 %copy-start.30 = (f32[256]{0:T(256)}, f32[256]{0:T(256)S(1)}, u32[]{:S(2)}) copy-start(f32[256]{0:T(256)S(1)} %add_rsqrt_fusion.1) | copy-start | bytes 3076
  68.3 132.7 %copy-start.2 = (bf16[32,4,8,128]{3,2,1,0:T(8,128)(2,1)}, bf16[32,4,8,128]{3,2,1,0:T(8,128)(2,1)S(1)}, u32[]{:S(2)}) copy-start(bf16[32,4,8,128]{3,2,1,0:T(8,128)(2,1)S(1)} %fusion.36) | copy-start | bytes 786436
  116.2 202.0 %all-gather.42.cloned.1.call-start = ((), (), s32[]{:S(2)}) async-start(), calls=%async_computation.12 | async-start | bytes 1310720 | tf_op jit(solution)/shard_map/all_gather | solution.py:14
  118.9 48.7 %copy-start.5 = (bf16[128,512]{1,0:T(8,128)(2,1)S(1)}, bf16[128,512]{1,0:T(8,128)(2,1)}, u32[]{:S(2)}) copy-start(bf16[128,512]{1,0:T(8,128)(2,1)} %param.32) | copy-start | bytes 393220
  119.5 64.3 %copy-start.37 = (u32[32]{0:T(128)S(1)}, u32[32]{0:T(128)}, u32[]{:S(2)}) copy-start(u32[32]{0:T(128)} %constant.215) | copy-start | bytes 388
  121.4 278.6 %all-gather.34.cloned.1.call-start = ((), (), s32[]{:S(2)}) async-start(), calls=%async_computation.7 | async-start | bytes 5242880 | tf_op jit(solution)/shard_map/all_gather | solution.py:208
  139.2 341.4 %all-gather.38.cloned.1.call-start = ((), (), s32[]{:S(2)}) async-start(), calls=%async_computation.9 | async-start | bytes 5242880 | tf_op jit(solution)/shard_map/all_gather | solution.py:210
  167.5 358.9 %all-gather.30.cloned.1.call-start = ((), (), s32[]{:S(2)}) async-start(), calls=%async_computation.5 | async-start | bytes 2621440 | tf_op jit(solution)/shard_map/all_gather | solution.py:209
  178.2 359.0 %reduce-scatter.2.cloned.1.call-start = ((), (), s32[]{:S(2)}) async-start(), calls=%async_computation.10 | async-start | bytes 1572864 | tf_op jit(solution)/shard_map/reduce_scatter | solution.py:312
  318.3 7.6 %copy-start.8 = (f32[1,2,4,128]{3,2,1,0:T(4,128)S(1)}, f32[1,2,4,128]{3,2,1,0:T(4,128)}, u32[]{:S(2)}) copy-start(f32[1,2,4,128]{3,2,1,0:T(4,128)} %param.29) | copy-start | bytes 12292
  318.3 7.6 %copy-start.29 = (f32[4]{0:T(128)S(1)}, f32[4]{0:T(128)}, u32[]{:S(2)}) copy-start(f32[4]{0:T(128)} %get-tuple-element.608) | copy-start | bytes 52
  318.3 7.6 %copy-start.32 = (f32[4]{0:T(128)S(1)}, f32[4]{0:T(128)}, u32[]{:S(2)}) copy-start(f32[4]{0:T(128)} %subtract_exponential_fusion.10) | copy-start | bytes 52
  326.6 1.1 copy-start.33
  327.4 6.7 %copy-start.1 = (bf16[4,256,256]{1,2,0:T(8,128)(2,1)S(1)}, bf16[4,256,256]{1,2,0:T(8,128)(2,1)}, u32[]{:S(2)}) copy-start(bf16[4,256,256]{1,2,0:T(8,128)(2,1)} %get-tuple-element.632) | copy-start | bytes 1572868
  334.1 65.9 %copy-start.31 = (f32[256]{0:T(256)S(1)}, f32[256]{0:T(256)}, u32[]{:S(2)}) copy-start(f32[256]{0:T(256)} %copy-done.30) | copy-start | bytes 3076
  334.1 65.9 %copy-start.35 = (f32[2048]{0:T(1024)S(1)}, f32[2048]{0:T(1024)}, u32[]{:S(2)}) copy-start(f32[2048]{0:T(1024)} %param.20) | copy-start | bytes 24580
  336.1 70.2 %copy-start.27 = (f32[4,128]{1,0:T(4,128)S(1)}, f32[4,128]{1,0:T(4,128)}, u32[]{:S(2)}) copy-start(f32[4,128]{1,0:T(4,128)} %param.30) | copy-start | bytes 6148
  403.5 77.2 %copy-start.9 = (s32[1024]{0:T(1024)S(1)}, s32[1024]{0:T(1024)}, u32[]{:S(2)}) copy-start(s32[1024]{0:T(1024)} %get-tuple-element.635) | copy-start | bytes 12292
  403.5 77.2 %copy-start.10 = (s32[1024]{0:T(1024)S(1)}, s32[1024]{0:T(1024)}, u32[]{:S(2)}) copy-start(s32[1024]{0:T(1024)} %get-tuple-element.636) | copy-start | bytes 12292
  403.5 77.2 %copy-start.11 = (f32[1024]{0:T(1024)S(1)}, f32[1024]{0:T(1024)}, u32[]{:S(2)}) copy-start(f32[1024]{0:T(1024)} %get-tuple-element.637) | copy-start | bytes 12292
  403.5 77.2 %copy-start.12 = (f32[1024]{0:T(1024)S(1)}, f32[1024]{0:T(1024)}, u32[]{:S(2)}) copy-start(f32[1024]{0:T(1024)} %get-tuple-element.638) | copy-start | bytes 12292
  403.5 77.2 %copy-start.13 = (f32[1024]{0:T(1024)S(1)}, f32[1024]{0:T(1024)}, u32[]{:S(2)}) copy-start(f32[1024]{0:T(1024)} %get-tuple-element.639) | copy-start | bytes 12292
  403.5 77.2 %copy-start.14 = (f32[1024]{0:T(1024)S(1)}, f32[1024]{0:T(1024)}, u32[]{:S(2)}) copy-start(f32[1024]{0:T(1024)} %get-tuple-element.640) | copy-start | bytes 12292
  403.5 77.2 %copy-start.15 = (f32[1024]{0:T(1024)S(1)}, f32[1024]{0:T(1024)}, u32[]{:S(2)}) copy-start(f32[1024]{0:T(1024)} %get-tuple-element.641) | copy-start | bytes 12292
  403.5 77.2 %copy-start.16 = (f32[1024]{0:T(1024)S(1)}, f32[1024]{0:T(1024)}, u32[]{:S(2)}) copy-start(f32[1024]{0:T(1024)} %get-tuple-element.642) | copy-start | bytes 12292
  403.6 77.2 %copy-start.17 = (f32[1024]{0:T(1024)S(1)}, f32[1024]{0:T(1024)}, u32[]{:S(2)}) copy-start(f32[1024]{0:T(1024)} %get-tuple-element.643) | copy-start | bytes 12292
  403.6 77.2 %copy-start.18 = (f32[1024]{0:T(1024)S(1)}, f32[1024]{0:T(1024)}, u32[]{:S(2)}) copy-start(f32[1024]{0:T(1024)} %get-tuple-element.644) | copy-start | bytes 12292
  403.6 77.2 %copy-start.19 = (f32[1024]{0:T(1024)S(1)}, f32[1024]{0:T(1024)}, u32[]{:S(2)}) copy-start(f32[1024]{0:T(1024)} %get-tuple-element.645) | copy-start | bytes 12292
  403.6 77.2 %copy-start.20 = (f32[1024]{0:T(1024)S(1)}, f32[1024]{0:T(1024)}, u32[]{:S(2)}) copy-start(f32[1024]{0:T(1024)} %get-tuple-element.646) | copy-start | bytes 12292
  403.6 77.2 %copy-start.21 = (f32[1024]{0:T(1024)S(1)}, f32[1024]{0:T(1024)}, u32[]{:S(2)}) copy-start(f32[1024]{0:T(1024)} %get-tuple-element.647) | copy-start | bytes 12292
  403.6 77.2 %copy-start.22 = (f32[1024]{0:T(1024)S(1)}, f32[1024]{0:T(1024)}, u32[]{:S(2)}) copy-start(f32[1024]{0:T(1024)} %get-tuple-element.648) | copy-start | bytes 12292
  403.6 77.2 %copy-start.23 = (f32[1024]{0:T(1024)S(1)}, f32[1024]{0:T(1024)}, u32[]{:S(2)}) copy-start(f32[1024]{0:T(1024)} %get-tuple-element.649) | copy-start | bytes 12292
  403.6 77.2 %copy-start.24 = (f32[1024]{0:T(1024)S(1)}, f32[1024]{0:T(1024)}, u32[]{:S(2)}) copy-start(f32[1024]{0:T(1024)} %get-tuple-element.650) | copy-start | bytes 12292
  403.6 77.2 %copy-start.25 = (f32[1024]{0:T(1024)S(1)}, f32[1024]{0:T(1024)}, u32[]{:S(2)}) copy-start(f32[1024]{0:T(1024)} %get-tuple-element.651) | copy-start | bytes 12292
  403.6 77.2 %copy-start.26 = (f32[1024]{0:T(1024)S(1)}, f32[1024]{0:T(1024)}, u32[]{:S(2)}) copy-start(f32[1024]{0:T(1024)} %get-tuple-element.652) | copy-start | bytes 12292
  403.7 77.2 %copy-start.36 = (s32[256]{0:T(256)S(1)}, s32[256]{0:T(256)}, u32[]{:S(2)}) copy-start(s32[256]{0:T(256)} %iota_add_fusion.1) | copy-start | bytes 3076
  403.7 2.8 collective-permute-start
  405.0 5.7 %collective-permute-start.1 = (bf16[8,1024]{1,0:T(8,128)(2,1)S(1)}, bf16[8,1024]{1,0:T(8,128)(2,1)S(1)}, u32[]{:S(2)}, u32[]{:S(2)}) collective-permute-start(bf16[8,1024]{1,0:T(8,128)(2,1)S(1)} %get-tuple-element.621), channel_id=1, source_target_pairs={{8,0},{16,8},{24,16},{9,1},{17,9},{25,17},{10,2},{18,10},{26,18},{... | collective-permute-start | bytes 49160 | tf_op jit(solution)/shard_map/ppermute | solution.py:36
Sparse Core Ops, SparseCore 0:
  20.0 45.9 all-gather.23
  67.5 44.4 all-gather.21
  113.8 25.3 all-gather.31
  140.9 26.4 all-gather.35
  168.9 46.0 all-gather.25
  216.4 44.4 all-gather.27
  262.5 26.7 all-gather.39
  290.9 27.3 all-gather.41
  319.8 80.1 all-gather.33
  401.4 79.2 all-gather.37
  482.2 44.1 all-gather.29
  529.9 7.1 reduce-scatter.1
where the time goes:
time: 545 us; the launch traced here: 544 us
  waiting for transfers between devices  359 us (66%)
  blocking collectives  93.4 us (17%)
  matrix products  34.2 us (6%)
  other arithmetic  26.8 us (5%)
  between operations  15 us (3%)
  local copies, waits for them, and re-layouts  12.1 us (2%)
    all_gather x1, waiting for transfers between devices, per_device(): lax.all_gather(line_pool_out, 'sp', axis=0, tiled=True)  69.9 us
    all_gather x1, waiting for transfers between devices, per_device(): lax.all_gather(line_pool, 'sp', axis=0, tiled=True)  63.9 us
    all_gather x1, waiting for transfers between devices, per_device(): lax.all_gather(line_value, 'sp', axis=0, tiled=True)  43.7 us
    all_gather x2, waiting for transfers between devices, carried_in(): everything = jax.tree.map(lambda part: lax.all_gather(part, axis), x)  42.1 us
    all_gather x1, waiting for transfers between devices, per_device(): lax.all_gather(line_mem_out, 'sp', axis=0, tiled=True)  40.3 us
    all_gather x1, waiting for transfers between devices, per_device(): lax.all_gather(line_outgate, 'sp', axis=0, tiled=True)  31.8 us
    all_gather x1, waiting for transfers between devices, per_device(): lax.all_gather(pool_out_weight, 'fs', axis=0, tiled=True)  28.2 us
    all_gather x2, blocking collectives, carried_in(): everything = jax.tree.map(lambda part: lax.all_gather(part, axis), x)  24.6 us
  transfers between devices with their start and end apart: 14, of which 12 were waited for; matrix products, arithmetic and copies ran while one was open for 13% of the time, Pallas kernels for 0%

commit v1 on v0

--- a/solution.py
+++ b/solution.py
@@ -7,6 +7,18 @@
 HALO = 8
 norm_eps = 1e-06
 exact_mode = lax.Precision.HIGHEST
+
+
+def doubled_up(shard, axis, dim):
+    ways, here, step = (lax.axis_size(axis), lax.axis_index(axis), shard.shape[dim])
+    line, have = (shard, 1)
+    while have < ways:
+        line = jnp.concatenate(
+            [line, lax.ppermute(line, axis, [(d, (d - have) % ways) for d in range(ways)])],
+            axis=dim,
+        )
+        have = 2 * have
+    return jnp.roll(line, here * step, axis=dim)
 
 
 def carried_in(x, axis, combine, identity, reverse):
@@ -204,7 +216,7 @@
         lax.all_gather(line_query, "sp", axis=0, tiled=True),
         lax.all_gather(line_key, "sp", axis=0, tiled=True),
         lax.all_gather(line_value, "sp", axis=0, tiled=True),
-        lax.all_gather(line_outgate, "sp", axis=0, tiled=True),
+        doubled_up(line_outgate, "sp", 0),
         lax.all_gather(line_pool, "sp", axis=0, tiled=True),
         lax.all_gather(line_mem_out, "sp", axis=0, tiled=True),
         lax.all_gather(line_pool_out, "sp", axis=0, tiled=True),

time: 545 us -> 544 us (level)
  waiting for transfers between devices: 359 us -> 317 us
  blocking collectives: 93.4 us -> 123 us
  starting transfers between devices: 3.03 us -> 9.97 us
    all_gather x2, waiting for transfers between devices: 42.1 us -> 0.02 us  [carried_in(): everything = jax.tree.map(lambda part: lax.all_gather(part, axis), x)]
    ppermute x0 -> x2, waiting for transfers between devices: none -> 35.3 us  [doubled_up(): lax.ppermute(line, axis, [(d, (d - have) % ways) for d in range(ways)])]
    all_gather x1 -> x0, waiting for transfers between devices: 31.8 us -> none  [per_device(): lax.all_gather(line_outgate, 'sp', axis=0, tiled=True)]
    unnamed x1, blocking collectives: 12.3 us -> 30.9 us
    all_gather x1, waiting for transfers between devices: 63.9 us -> 48.5 us  [per_device(): lax.all_gather(line_pool, 'sp', axis=0, tiled=True)]
    all_gather x2, blocking collectives: 24.6 us -> 37.6 us  [carried_in(): everything = jax.tree.map(lambda part: lax.all_gather(part, axis), x)]
    all_gather x1, waiting for transfers between devices: 8.72 us -> 20.2 us  [per_device(): lax.all_gather(line_key, 'sp', axis=0, tiled=True)]
    ppermute x0 -> x2, starting transfers between devices: none -> 6.96 us  [doubled_up(): lax.ppermute(line, axis, [(d, (d - have) % ways) for d in range(ways)])]
  transfers between devices with their start and end apart: 14 -> 15, of which waited for: 12 -> 11; matrix products, arithmetic and copies ran while one was open for 13% -> 13% of each run, Pallas kernels for 0% -> 0%
where the time goes in v1:
time: 544 us; the launch traced here: 542 us
  waiting for transfers between devices  317 us (58%)
  blocking collectives  123 us (23%)
  matrix products  32.8 us (6%)
  other arithmetic  28 us (5%)
  local copies, waits for them, and re-layouts  15.9 us (3%)
  between operations  14.7 us (3%)
  starting transfers between devices  9.97 us (2%)
    all_gather x1, waiting for transfers between devices, per_device(): lax.all_gather(line_pool_out, 'sp', axis=0, tiled=True)  70 us
    all_gather x1, waiting for transfers between devices, per_device(): lax.all_gather(line_pool, 'sp', axis=0, tiled=True)  48.5 us
    all_gather x1, waiting for transfers between devices, per_device(): lax.all_gather(line_value, 'sp', axis=0, tiled=True)  43.7 us
    all_gather x1, waiting for transfers between devices, per_device(): lax.all_gather(line_mem_out, 'sp', axis=0, tiled=True)  40.1 us
    all_gather x2, blocking collectives, carried_in(): everything = jax.tree.map(lambda part: lax.all_gather(part, axis), x)  37.6 us
    ppermute x2, waiting for transfers between devices, doubled_up(): lax.ppermute(line, axis, [(d, (d - have) % ways) for d in range(ways)])  35.3 us
    unnamed x1, blocking collectives  30.9 us
    all_gather x1, waiting for transfers between devices, per_device(): lax.all_gather(pool_out_weight, 'fs', axis=0, tiled=True)  28.2 us
  transfers between devices with their start and end apart: 15, of which 11 were waited for; matrix products, arithmetic and copies ran while one was open for 13% of the time, Pallas kernels for 0%

profile of v1, /device:TPU:0, one launch (start us, length us, event | category | flops | bytes accessed | tf_op | source)
XLA Modules:
  0.0 541.8 jit_solution(12215091409018974371)
XLA Ops:
  6.6 13.3 %all_gather.86 = bf16[512,512]{1,0:T(8,128)(2,1)} all-gather(bf16[128,512]{1,0:T(8,128)(2,1)} %param.22), channel_id=1, replica_groups=mesh['sp'=4,'fs'=4,'tp'=2] {'fs'}, dimensions={0}, use_global_device_ids=true | all-gather | bytes 655360 | tf_op jit(solution)/shard_map/all_gather | solution.py:208
  20.0 11.4 %all_gather.84 = bf16[512,512]{1,0:T(8,128)(2,1)} all-gather(bf16[128,512]{1,0:T(8,128)(2,1)} %param.23), channel_id=1, replica_groups=mesh['sp'=4,'fs'=4,'tp'=2] {'fs'}, dimensions={0}, use_global_device_ids=true | all-gather | bytes 655360 | tf_op jit(solution)/shard_map/all_gather | solution.py:209
  31.5 0.7 all-gather.29.cloned.1.call-update
  32.8 9.8 %all_gather.92 = bf16[512,512]{1,0:T(8,128)(2,1)} all-gather(bf16[128,512]{1,0:T(8,128)(2,1)S(1)} %copy-done.5), channel_id=1, replica_groups=mesh['sp'=4,'fs'=4,'tp'=2] {'fs'}, dimensions={0}, use_global_device_ids=true | all-gather | bytes 655360 | tf_op jit(solution)/shard_map/all_gather | solution.py:207
  43.7 1.2 reduce-window.24
  45.8 20.2 %all-gather.23.cloned.1.call-done = bf16[2048,512]{1,0:T(8,128)(2,1)} async-done(((bf16[512,512]{1,0:T(8,128)(2,1)}), bf16[2048,512]{1,0:T(8,128)(2,1)}) %all-gather.23.cloned.1.call-update) | async-done | bytes 2097168 | tf_op jit(solution)/shard_map/all_gather | solution.py:217
  66.0 2.3 fusion.51
  68.3 43.7 %all-gather.21.cloned.1.call-done = bf16[2048,512]{1,0:T(8,128)(2,1)} async-done(((bf16[512,512]{1,0:T(8,128)(2,1)}), bf16[2048,512]{1,0:T(8,128)(2,1)}) %all-gather.21.cloned.1.call-update) | async-done | bytes 2097168 | tf_op jit(solution)/shard_map/all_gather | solution.py:218
  112.1 2.3 fusion.50
  114.4 1.9 fusion.86
  116.6 1.2 reduce-window.26
  119.6 1.9 fusion.80
  121.5 17.8 %all-gather.29.cloned.1.call-done = bf16[512,1024]{1,0:T(8,128)(2,1)} async-done(((bf16[128,1024]{1,0:T(8,128)(2,1)}), bf16[512,1024]{1,0:T(8,128)(2,1)}) %all-gather.29.cloned.1.call-update) | async-done | bytes 1048592 | tf_op jit(solution)/shard_map/all_gather | solution.py:211
  139.4 28.2 %all-gather.33.cloned.1.call-done = bf16[512,1024]{1,0:T(8,128)(2,1)} async-done(((bf16[128,1024]{1,0:T(8,128)(2,1)}), bf16[512,1024]{1,0:T(8,128)(2,1)}) %all-gather.33.cloned.1.call-update) | async-done | bytes 1048592 | tf_op jit(solution)/shard_map/all_gather | solution.py:213
  167.6 10.1 %all_gather.101 = bf16[512,512]{1,0:T(8,128)(2,1)S(1)} all-gather(bf16[128,512]{1,0:T(8,128)(2,1)S(1)} %copy-done.6), channel_id=1, replica_groups=mesh['sp'=4,'fs'=4,'tp'=2] {'fs'}, dimensions={0}, use_global_device_ids=true | all-gather | bytes 655360 | tf_op jit(solution)/shard_map/all_gather | solution.py:210
  177.7 3.3 collective-permute-start
  181.0 10.5 %all_gather.102 = bf16[512,512]{1,0:T(8,128)(2,1)} all-gather(bf16[128,512]{1,0:T(8,128)(2,1)S(1)} %copy-done.7), channel_id=1, replica_groups=mesh['sp'=4,'fs'=4,'tp'=2] {'fs'}, dimensions={0}, use_global_device_ids=true | all-gather | bytes 655360 | tf_op jit(solution)/shard_map/all_gather | solution.py:212
  194.6 17.9 %collective-permute-done = bf16[512,512]{1,0:T(8,128)(2,1)S(1)} collective-permute-done((bf16[512,512]{1,0:T(8,128)(2,1)S(1)}, bf16[512,512]{1,0:T(8,128)(2,1)S(1)}, u32[]{:S(2)}, u32[]{:S(2)}) %collective-permute-start) | collective-permute-done | bytes 524320 | tf_op jit(solution)/shard_map/ppermute | solution.py:17
  212.5 1.1 pad_maximum_fusion
  213.6 3.6 collective-permute-start.1
  220.0 30.9 %all-reduce.4 = (f32[16]{0:T(128)S(1)}, f32[16]{0:T(128)S(1)}, f32[16]{0:T(128)S(1)}, f32[16]{0:T(128)S(1)}) all-reduce(f32[16]{0:T(128)S(1)} %dynamic-update-slice.2, f32[16]{0:T(128)S(1)} %dynamic-update-slice.3, f32[16]{0:T(128)S(1)} %dynamic-update-slice, f32[16]{0:T(128)S(1)} %dynamic-update-slice.1), channel_id=6, replica_groups=mesh['sp'=4,'fs'=4,'tp'=2] {'sp'}, use_global_device_ids=true, to_apply=%add.2 | all-reduce | flops 64 | bytes 512
  250.9 0.7 reshape.473
  254.9 0.7 fusion.73
  255.6 17.4 %collective-permute-done.1 = bf16[1024,512]{1,0:T(8,128)(2,1)S(1)} collective-permute-done((bf16[1024,512]{1,0:T(8,128)(2,1)}, bf16[1024,512]{1,0:T(8,128)(2,1)S(1)}, u32[]{:S(2)}, u32[]{:S(2)}) %collective-permute-start.1) | collective-permute-done | bytes 1048608 | tf_op jit(solution)/shard_map/ppermute | solution.py:17
  273.4 1.0 copy-done.1
  274.4 0.8 fusion.47
  275.4 1.3 fusion.85
  276.8 25.1 %all-gather.8 = f32[4,4,128]{2,1,0:T(4,128)S(1)} all-gather(f32[1,4,128]{2,1,0:T(4,128)S(1)} %bitcast.305), channel_id=5, replica_groups=mesh['sp'=4,'fs'=4,'tp'=2] {'sp'}, dimensions={0}, use_global_device_ids=true | all-gather | bytes 10240 | tf_op jit(solution)/shard_map/all_gather | solution.py:26
  302.2 12.5 %all-gather.9 = f32[4,4,128]{2,1,0:T(4,128)S(1)} all-gather(f32[1,4,128]{2,1,0:T(4,128)S(1)} %bitcast.301), channel_id=9, replica_groups=mesh['sp'=4,'fs'=4,'tp'=2] {'sp'}, dimensions={0}, use_global_device_ids=true | all-gather | bytes 10240 | tf_op jit(solution)/shard_map/all_gather | solution.py:26
  314.7 2.4 fusion.52
  317.1 0.7 copy.134
  317.8 3.2 rev.25
  321.0 7.5 %while.12 = (s32[]{:T(128)}, f32[4,128,128]{2,1,0:T(8,128)S(1)}, f32[4,128]{1,0:T(4,128)S(1)}, f32[4]{0:T(128)S(1)}, f32[4]{0:T(128)S(1)}, /*index=5*/s32[]{:T(1...) while((s32[]{:T(128)}, f32[4,128,128]{2,1,0:T(8,128)S(1)}, ...), condition=%wide.region_5.6_spmd.clone, body=%wide.region_4.5_spmd.clone.sunk | while | flops 330284 | bytes 792973 | solution.py:37
  321.1 0.7 broadcast_select_fusion.10
  321.8 1.1 fusion.172
  322.9 0.7 broadcast_select_fusion.10
  323.6 1.1 fusion.172
  324.8 0.7 broadcast_select_fusion.10
  325.5 1.1 fusion.172
  326.7 0.7 broadcast_select_fusion.10
  327.4 1.1 fusion.172
  329.7 2.2 fusion.149
  331.9 7.4 %while.13 = (s32[]{:T(128)}, f32[4,128,128]{2,1,0:T(8,128)S(1)}, f32[4,128]{1,0:T(4,128)S(1)}, f32[4]{0:T(128)S(1)}, f32[4]{0:T(128)S(1)}, /*index=5*/s32[]{:T(1...) while((s32[]{:T(128)}, f32[4,128,128]{2,1,0:T(8,128)S(1)}, ...), condition=%wide.region_12.13_spmd.clone, body=%wide.region_11.12_spmd.clone.sunk | while | flops 330288 | bytes 793035 | solution.py:37
  331.9 0.7 broadcast_select_fusion.11
  332.6 1.1 fusion.174
  333.8 0.7 broadcast_select_fusion.11
  334.5 1.1 fusion.174
  335.6 0.7 broadcast_select_fusion.11
  336.3 1.1 fusion.174
  337.5 0.7 broadcast_select_fusion.11
  338.2 1.1 fusion.174
  341.2 1.2 fusion.27
  342.5 5.1 rev.26
  347.9 1.7 multiply_reduce_fusion
  349.6 48.5 %all-gather.31.cloned.1.call-done = bf16[2048,1024]{1,0:T(8,128)(2,1)} async-done(((bf16[512,1024]{1,0:T(8,128)(2,1)}), bf16[2048,1024]{1,0:T(8,128)(2,1)}) %all-gather.31.cloned.1.call-update) | async-done | bytes 4194320 | tf_op jit(solution)/shard_map/all_gather | solution.py:220
  398.1 3.5 convolution_convert_fusion
  401.8 1.3 collective-permute-start.2
  403.1 1.3 collective-permute-start.3
  404.5 4.2 collective-permute-done.3
  408.9 70.0 %all-gather.35.cloned.1.call-done = bf16[2048,1024]{1,0:T(8,128)(2,1)} async-done(((bf16[512,1024]{1,0:T(8,128)(2,1)}), bf16[2048,1024]{1,0:T(8,128)(2,1)}) %all-gather.35.cloned.1.call-update) | async-done | bytes 4194320 | tf_op jit(solution)/shard_map/all_gather | solution.py:222
  479.1 5.3 fusion.89
  484.4 40.1 %all-gather.27.cloned.1.call-done = bf16[2048,512]{1,0:T(8,128)(2,1)} async-done(((bf16[512,512]{1,0:T(8,128)(2,1)}), bf16[2048,512]{1,0:T(8,128)(2,1)}) %all-gather.27.cloned.1.call-update) | async-done | bytes 2097168 | tf_op jit(solution)/shard_map/all_gather | solution.py:221
  524.5 3.4 fusion.16
  527.9 7.3 %reduce-scatter.2.cloned.1.call-done = bf16[128,2048]{1,0:T(8,128)(2,1)} async-done(((bf16[256,2048]{1,0:T(8,128)(2,1)}), bf16[128,2048]{1,0:T(8,128)(2,1)}) %reduce-scatter.2.cloned.1.call-update) | async-done | bytes 524304 | tf_op jit(solution)/shard_map/reduce_scatter | solution.py:324
  (220 shorter events, 18.6 us)
Async XLA Ops:
  6.5 26.3 %copy-start.5 = (bf16[128,512]{1,0:T(8,128)(2,1)S(1)}, bf16[128,512]{1,0:T(8,128)(2,1)}, u32[]{:S(2)}) copy-start(bf16[128,512]{1,0:T(8,128)(2,1)} %param.21) | copy-start | bytes 393220
  6.5 36.1 %copy-start.8 = (bf16[4,4,2048]{2,1,0:T(4,128)(2,1)S(1)}, bf16[4,4,2048]{2,1,0:T(4,128)(2,1)}, u32[]{:S(2)}) copy-start(bf16[4,4,2048]{2,1,0:T(4,128)(2,1)} %param.25) | copy-start | bytes 196612
  6.5 36.2 %copy-start.30 = (f32[4,4]{1,0:T(4,128)S(1)}, f32[4,4]{1,0:T(4,128)}, u32[]{:S(2)}) copy-start(f32[4,4]{1,0:T(4,128)} %param.26) | copy-start | bytes 196
  6.5 36.3 %copy-start = (bf16[1,256,2048]{2,1,0:T(8,128)(2,1)S(1)}, bf16[1,256,2048]{2,1,0:T(8,128)(2,1)}, u32[]{:S(2)}) copy-start(bf16[1,256,2048]{2,1,0:T(8,128)(2,1)} %param.19) | copy-start | bytes 3145732
  6.5 59.4 %all-gather.23.cloned.1.call-start = ((), (), s32[]{:S(2)}) async-start(), calls=%async_computation.2 | async-start | bytes 2621440 | tf_op jit(solution)/shard_map/all_gather | solution.py:217
  19.9 23.2 %copy-start.37 = (f32[2048]{0:T(1024)S(1)}, f32[2048]{0:T(1024)}, u32[]{:S(2)}) copy-start(f32[2048]{0:T(1024)} %param.20) | copy-start | bytes 24580
  19.9 92.1 %all-gather.21.cloned.1.call-start = ((), (), s32[]{:S(2)}) async-start(), calls=%async_computation.1 | async-start | bytes 2621440 | tf_op jit(solution)/shard_map/all_gather | solution.py:218
  31.4 107.9 %all-gather.29.cloned.1.call-start = ((), (), s32[]{:S(2)}) async-start(), calls=%async_computation.5 | async-start | bytes 1310720 | tf_op jit(solution)/shard_map/all_gather | solution.py:211
  32.2 135.4 %all-gather.33.cloned.1.call-start = ((), (), s32[]{:S(2)}) async-start(), calls=%async_computation.7 | async-start | bytes 1310720 | tf_op jit(solution)/shard_map/all_gather | solution.py:213
  32.7 10.9 %slice-start = ((f32[1,2,4,256]{3,2,1,0:T(4,128)}), f32[1,1,4,256]{3,2,1,0:T(4,128)S(1)}, s32[]{:S(2)}) async-start(f32[1,2,4,256]{3,2,1,0:T(4,128)} %param.27), calls=%async_computation.12 | async-start | bytes 8192 | tf_op jit(solution)/shard_map/slice | solution.py:247
  32.7 12.9 %copy-start.9 = (f32[1,2,4,256]{3,2,1,0:T(4,128)S(1)}, f32[1,2,4,256]{3,2,1,0:T(4,128)}, u32[]{:S(2)}) copy-start(f32[1,2,4,256]{3,2,1,0:T(4,128)} %param.27) | copy-start | bytes 24580
  32.8 282.0 %all-gather.25.cloned.1.call-start = ((), (), s32[]{:S(2)}) async-start(), calls=%async_computation.3 | async-start | bytes 2621440 | tf_op jit(solution)/shard_map/all_gather | solution.py:216
  42.6 278.4 %all-gather.37.cloned.1.call-start = ((), (), s32[]{:S(2)}) async-start(), calls=%async_computation.10 | async-start | bytes 1310720 | tf_op jit(solution)/shard_map/all_gather | solution.py:26
  43.1 68.9 %copy-start.32 = (f32[256]{0:T(256)}, f32[256]{0:T(256)S(1)}, u32[]{:S(2)}) copy-start(f32[256]{0:T(256)S(1)} %add_rsqrt_fusion.1) | copy-start | bytes 3076
  68.3 99.3 %copy-start.4 = (bf16[32,4,8,128]{3,2,1,0:T(8,128)(2,1)}, bf16[32,4,8,128]{3,2,1,0:T(8,128)(2,1)S(1)}, u32[]{:S(2)}) copy-start(bf16[32,4,8,128]{3,2,1,0:T(8,128)(2,1)S(1)} %fusion.51) | copy-start | bytes 786436
  116.3 215.6 %all-gather.39.cloned.1.call-start = ((), (), s32[]{:S(2)}) async-start(), calls=%async_computation.11 | async-start | bytes 1310720 | tf_op jit(solution)/shard_map/all_gather | solution.py:26
  118.9 48.7 %copy-start.6 = (bf16[128,512]{1,0:T(8,128)(2,1)S(1)}, bf16[128,512]{1,0:T(8,128)(2,1)}, u32[]{:S(2)}) copy-start(bf16[128,512]{1,0:T(8,128)(2,1)} %param.24) | copy-start | bytes 393220
  119.3 61.8 %copy-start.7 = (bf16[128,512]{1,0:T(8,128)(2,1)S(1)}, bf16[128,512]{1,0:T(8,128)(2,1)}, u32[]{:S(2)}) copy-start(bf16[128,512]{1,0:T(8,128)(2,1)} %param.32) | copy-start | bytes 393220
  121.5 276.6 %all-gather.31.cloned.1.call-start = ((), (), s32[]{:S(2)}) async-start(), calls=%async_computation.6 | async-start | bytes 5242880 | tf_op jit(solution)/shard_map/all_gather | solution.py:220
  139.3 339.6 %all-gather.35.cloned.1.call-start = ((), (), s32[]{:S(2)}) async-start(), calls=%async_computation.8 | async-start | bytes 5242880 | tf_op jit(solution)/shard_map/all_gather | solution.py:222
  167.5 50.3 %copy-start.41 = (u32[32]{0:T(128)S(1)}, u32[32]{0:T(128)}, u32[]{:S(2)}) copy-start(u32[32]{0:T(128)} %constant.237) | copy-start | bytes 388
  167.6 356.9 %all-gather.27.cloned.1.call-start = ((), (), s32[]{:S(2)}) async-start(), calls=%async_computation.4 | async-start | bytes 2621440 | tf_op jit(solution)/shard_map/all_gather | solution.py:221
  177.7 34.8 %collective-permute-start = (bf16[512,512]{1,0:T(8,128)(2,1)S(1)}, bf16[512,512]{1,0:T(8,128)(2,1)S(1)}, u32[]{:S(2)}, u32[]{:S(2)}) collective-permute-start(bf16[512,512]{1,0:T(8,128)(2,1)S(1)} %all_gather.101), channel_id=1, source_target_pairs={{0,24},{8,0},{16,8},{24,16},{1,25},{9,1},{17,9},{25,17},{2,26},{10... | collective-permute-start | bytes 1572872 | tf_op jit(solution)/shard_map/ppermute | solution.py:17
  191.5 343.7 %reduce-scatter.2.cloned.1.call-start = ((), (), s32[]{:S(2)}) async-start(), calls=%async_computation.9 | async-start | bytes 1572864 | tf_op jit(solution)/shard_map/reduce_scatter | solution.py:324
  213.6 59.5 %collective-permute-start.1 = (bf16[1024,512]{1,0:T(8,128)(2,1)}, bf16[1024,512]{1,0:T(8,128)(2,1)S(1)}, u32[]{:S(2)}, u32[]{:S(2)}) collective-permute-start(bf16[1024,512]{1,0:T(8,128)(2,1)} %pad_maximum_fusion), channel_id=1, source_target_pairs={{0,16},{8,24},{16,0},{24,8},{1,17},{9,25},{17,1},{25,9},{2,18},{10... | collective-permute-start | bytes 3145736 | tf_op jit(solution)/shard_map/ppermute | solution.py:17
  273.2 1.2 copy-start.1
  273.2 1.2 copy-start.33
  273.2 1.2 copy-start.38
  274.4 40.3 %copy-start.2 = (bf16[1,256,2048]{2,1,0:T(8,128)(2,1)S(1)}, bf16[1,256,2048]{2,1,0:T(8,128)(2,1)}, u32[]{:S(2)}) copy-start(bf16[1,256,2048]{2,1,0:T(8,128)(2,1)} %param.19) | copy-start | bytes 3145732
  331.9 7.5 %copy-start.10 = (f32[1,2,4,128]{3,2,1,0:T(4,128)S(1)}, f32[1,2,4,128]{3,2,1,0:T(4,128)}, u32[]{:S(2)}) copy-start(f32[1,2,4,128]{3,2,1,0:T(4,128)} %param.29) | copy-start | bytes 12292
  331.9 7.5 %copy-start.31 = (f32[4]{0:T(128)S(1)}, f32[4]{0:T(128)}, u32[]{:S(2)}) copy-start(f32[4]{0:T(128)} %get-tuple-element.608) | copy-start | bytes 52
  331.9 7.5 %copy-start.35 = (f32[4]{0:T(128)S(1)}, f32[4]{0:T(128)}, u32[]{:S(2)}) copy-start(f32[4]{0:T(128)} %subtract_exponential_fusion.10) | copy-start | bytes 52
  340.2 1.1 copy-start.36
  341.0 6.6 %copy-start.3 = (bf16[4,256,256]{1,2,0:T(8,128)(2,1)S(1)}, bf16[4,256,256]{1,2,0:T(8,128)(2,1)}, u32[]{:S(2)}) copy-start(bf16[4,256,256]{1,2,0:T(8,128)(2,1)} %get-tuple-element.632) | copy-start | bytes 1572868
  347.6 50.5 %copy-start.34 = (f32[256]{0:T(256)S(1)}, f32[256]{0:T(256)}, u32[]{:S(2)}) copy-start(f32[256]{0:T(256)} %copy-done.32) | copy-start | bytes 3076
  347.6 50.5 %copy-start.39 = (f32[2048]{0:T(1024)S(1)}, f32[2048]{0:T(1024)}, u32[]{:S(2)}) copy-start(f32[2048]{0:T(1024)} %param.20) | copy-start | bytes 24580
  349.6 54.8 %copy-start.29 = (f32[4,128]{1,0:T(4,128)S(1)}, f32[4,128]{1,0:T(4,128)}, u32[]{:S(2)}) copy-start(f32[4,128]{1,0:T(4,128)} %param.30) | copy-start | bytes 6148
  401.6 77.3 %copy-start.11 = (s32[1024]{0:T(1024)S(1)}, s32[1024]{0:T(1024)}, u32[]{:S(2)}) copy-start(s32[1024]{0:T(1024)} %get-tuple-element.635) | copy-start | bytes 12292
  401.6 77.3 %copy-start.12 = (s32[1024]{0:T(1024)S(1)}, s32[1024]{0:T(1024)}, u32[]{:S(2)}) copy-start(s32[1024]{0:T(1024)} %get-tuple-element.636) | copy-start | bytes 12292
  401.6 77.3 %copy-start.13 = (f32[1024]{0:T(1024)S(1)}, f32[1024]{0:T(1024)}, u32[]{:S(2)}) copy-start(f32[1024]{0:T(1024)} %get-tuple-element.637) | copy-start | bytes 12292
  401.6 77.3 %copy-start.14 = (f32[1024]{0:T(1024)S(1)}, f32[1024]{0:T(1024)}, u32[]{:S(2)}) copy-start(f32[1024]{0:T(1024)} %get-tuple-element.638) | copy-start | bytes 12292
  401.6 77.3 %copy-start.15 = (f32[1024]{0:T(1024)S(1)}, f32[1024]{0:T(1024)}, u32[]{:S(2)}) copy-start(f32[1024]{0:T(1024)} %get-tuple-element.639) | copy-start | bytes 12292
  401.6 77.3 %copy-start.16 = (f32[1024]{0:T(1024)S(1)}, f32[1024]{0:T(1024)}, u32[]{:S(2)}) copy-start(f32[1024]{0:T(1024)} %get-tuple-element.640) | copy-start | bytes 12292
  401.6 77.3 %copy-start.17 = (f32[1024]{0:T(1024)S(1)}, f32[1024]{0:T(1024)}, u32[]{:S(2)}) copy-start(f32[1024]{0:T(1024)} %get-tuple-element.641) | copy-start | bytes 12292
  401.7 77.3 %copy-start.18 = (f32[1024]{0:T(1024)S(1)}, f32[1024]{0:T(1024)}, u32[]{:S(2)}) copy-start(f32[1024]{0:T(1024)} %get-tuple-element.642) | copy-start | bytes 12292
  401.7 77.3 %copy-start.19 = (f32[1024]{0:T(1024)S(1)}, f32[1024]{0:T(1024)}, u32[]{:S(2)}) copy-start(f32[1024]{0:T(1024)} %get-tuple-element.643) | copy-start | bytes 12292
  401.7 77.3 %copy-start.20 = (f32[1024]{0:T(1024)S(1)}, f32[1024]{0:T(1024)}, u32[]{:S(2)}) copy-start(f32[1024]{0:T(1024)} %get-tuple-element.644) | copy-start | bytes 12292
  401.7 77.3 %copy-start.21 = (f32[1024]{0:T(1024)S(1)}, f32[1024]{0:T(1024)}, u32[]{:S(2)}) copy-start(f32[1024]{0:T(1024)} %get-tuple-element.645) | copy-start | bytes 12292
  401.7 77.3 %copy-start.22 = (f32[1024]{0:T(1024)S(1)}, f32[1024]{0:T(1024)}, u32[]{:S(2)}) copy-start(f32[1024]{0:T(1024)} %get-tuple-element.646) | copy-start | bytes 12292
  401.7 77.3 %copy-start.23 = (f32[1024]{0:T(1024)S(1)}, f32[1024]{0:T(1024)}, u32[]{:S(2)}) copy-start(f32[1024]{0:T(1024)} %get-tuple-element.647) | copy-start | bytes 12292
  401.7 77.3 %copy-start.24 = (f32[1024]{0:T(1024)S(1)}, f32[1024]{0:T(1024)}, u32[]{:S(2)}) copy-start(f32[1024]{0:T(1024)} %get-tuple-element.648) | copy-start | bytes 12292
  401.7 77.3 %copy-start.25 = (f32[1024]{0:T(1024)S(1)}, f32[1024]{0:T(1024)}, u32[]{:S(2)}) copy-start(f32[1024]{0:T(1024)} %get-tuple-element.649) | copy-start | bytes 12292
  401.7 77.3 %copy-start.26 = (f32[1024]{0:T(1024)S(1)}, f32[1024]{0:T(1024)}, u32[]{:S(2)}) copy-start(f32[1024]{0:T(1024)} %get-tuple-element.650) | copy-start | bytes 12292
  401.7 77.3 %copy-start.27 = (f32[1024]{0:T(1024)S(1)}, f32[1024]{0:T(1024)}, u32[]{:S(2)}) copy-start(f32[1024]{0:T(1024)} %get-tuple-element.651) | copy-start | bytes 12292
  401.8 77.3 %copy-start.28 = (f32[1024]{0:T(1024)S(1)}, f32[1024]{0:T(1024)}, u32[]{:S(2)}) copy-start(f32[1024]{0:T(1024)} %get-tuple-element.652) | copy-start | bytes 12292
  401.8 77.3 %copy-start.40 = (s32[256]{0:T(256)S(1)}, s32[256]{0:T(256)}, u32[]{:S(2)}) copy-start(s32[256]{0:T(256)} %iota_add_fusion.1) | copy-start | bytes 3076
  401.8 2.8 collective-permute-start.2
  403.1 5.7 %collective-permute-start.3 = (bf16[8,1024]{1,0:T(8,128)(2,1)S(1)}, bf16[8,1024]{1,0:T(8,128)(2,1)S(1)}, u32[]{:S(2)}, u32[]{:S(2)}) collective-permute-start(bf16[8,1024]{1,0:T(8,128)(2,1)S(1)} %get-tuple-element.621), channel_id=1, source_target_pairs={{8,0},{16,8},{24,16},{9,1},{17,9},{25,17},{10,2},{18,10},{26,18},{... | collective-permute-start | bytes 49160 | tf_op jit(solution)/shard_map/ppermute | solution.py:48
Sparse Core Ops, SparseCore 0:
  20.0 45.9 all-gather.22
  67.6 44.4 all-gather.20
  113.9 25.3 all-gather.28
  141.0 26.4 all-gather.32
  168.9 83.6 all-gather.24
  254.1 31.9 all-gather.36
  287.6 28.6 all-gather.38
  317.9 80.1 all-gather.30
  399.7 79.1 all-gather.34
  480.3 44.1 all-gather.26
  528.0 7.1 reduce-scatter.1
